TPU v7x, 32 devices: a whole 2x2x4 slice. The times are simulated.
32 devices in a mesh: rep: 2 (over x), fs: 4 (over z), tp: 4 (over y, core).
Axes of the slice: x: 2, y: 2, z: 4, core: 2. Of those that a mesh axis runs over, the one named last changes fastest.
Arguments:
- tokens: bfloat16 [4096, 2048], P(('rep', 'fs', 'tp')), may hold values from -6 to 6
- norm1_gain: float32 [2048], replicated, may hold values from 0.1 to 1.9
- in_weight: bfloat16 [2048, 1024], P('fs', 'tp'), may hold values from -0.125 to 0.125
- group_weight: bfloat16 [8, 128, 128], P('tp'), may hold values from -0.5 to 0.5
- pool_scale: float32 [1024], P('tp'), may hold values from 0.1 to 1.9
- out_weight: bfloat16 [1024, 2048], P('tp', 'fs'), may hold values from -0.1875 to 0.1875
- norm2_gain: float32 [2048], replicated, may hold values from 0.1 to 1.9
- up_weight: bfloat16 [2048, 8192], P('fs', 'tp'), may hold values from -0.125 to 0.125
- down_weight: bfloat16 [8192, 2048], P('tp', 'fs'), may hold values from -0.0625 to 0.0625
Outputs:
- layer_out: bfloat16 [4096, 2048], P(('rep', 'fs', 'tp'))
All inputs are finite; a program needn't handle non-finite values.
Results may differ from a plain program's by a relative error of at most 0.02.
Values may be sent and summed in bfloat16 or wider, within the bound.
A program may use at most 128 MiB of HBM per device.

v0:
```python
import functools

import jax
import jax.numpy as jnp
from jax import lax
from jax.experimental import pallas as pl
from jax.experimental.pallas import tpu as pltpu
from jax.sharding import PartitionSpec as P

MESH = pl.DeviceIdType.MESH
CHUNK_BYTES = 256 * 1024
LEVELS = 4

epsilon = 1e-06


def chunks_of(rows, columns, parts):
    count = max(1, rows * columns * 2 // parts // CHUNK_BYTES)
    while (rows // parts) % (count * 16):
        count -= 1
    return count


def dot(a, b):
    return jnp.dot(a, b, preferred_element_type=jnp.float32)


def tile_of(columns, most):
    tile = min(columns, most)
    while columns % tile:
        tile //= 2
    return tile


def kernel(
    sizes,
    tokens,
    gain1,
    in_hbm,
    group_weight,
    pool_scale,
    out_hbm,
    gain2,
    up_hbm,
    down_hbm,
    result,
    in_buf,
    out_buf,
    up_buf,
    down_buf,
    normed,
    projected,
    pool_out,
    mix_send,
    mix_recv,
    stream2,
    normed2,
    upper,
    hidden,
    sum_send,
    sum_recv,
    local_sem,
    in_sems,
    out_sems,
    up_sems,
    down_sems,
    tp_send,
    tp_recv,
):
    n_rep, n_fs, n_tp = sizes
    r, f, t = lax.axis_index("rep"), lax.axis_index("fs"), lax.axis_index("tp")
    rows = tokens.shape[0]
    length = rows * n_tp
    width = tokens.shape[1]
    part = width // n_fs
    buffers = (in_buf, out_buf, up_buf, down_buf)
    sources = (in_hbm, out_hbm, up_hbm, down_hbm)
    sems = (
        in_sems,
        out_sems,
        up_sems,
        down_sems,
    )
    chunk_counts = [chunks_of(b.shape[1], b.shape[2], n_rep) for b in buffers]

    loads = []
    for index in range(4):
        load = pltpu.make_async_copy(sources[index], buffers[index].at[f], local_sem.at[index])
        load.start()
        loads.append(load)

    barrier = pltpu.get_barrier_semaphore()
    greeted = [{"fs": lax.rem(f + d, n_fs)} for d in (1, n_fs - 1)]
    greeted += [{"rep": lax.rem(r + d, n_rep)} for d in range(1, n_rep)]
    greeted += [{"tp": lax.rem(t + d, n_tp)} for d in range(1, n_tp)]
    for device in greeted:
        pl.semaphore_signal(barrier, inc=1, device_id=device, device_id_type=MESH)

    def order(p):
        nearest = jnp.minimum(f, n_fs - 1 - f)
        step = (p + 1) // 2
        near = f + step if p % 2 else f - step
        far = f + (p - nearest) * jnp.where(2 * f < n_fs, 1, -1)
        return jnp.where(p <= 2 * nearest, near, far)

    def piece(g, j, q, c):
        buf = buffers[g]
        size = buf.shape[1] // n_rep // chunk_counts[g]
        start = pl.multiple_of((q * chunk_counts[g] + c) * size, size)
        return buf.at[j, pl.ds(start, size), :]

    def remote(g, j, q, c, send_slot, device):
        block = piece(g, j, q, c)
        return pltpu.make_async_remote_copy(
            src_ref=block,
            dst_ref=block,
            send_sem=sems[g].at[j, send_slot, c],
            recv_sem=sems[g].at[j, q, c],
            device_id=device,
            device_id_type=MESH,
        )

    def along(g, j, c, way, act):
        if way == 0:

            @pl.when(f > 0)
            def _():
                act(remote(g, j, r, c, 2 * n_rep, {"fs": f - 1}))

        else:

            @pl.when(f < n_fs - 1)
            def _():
                act(remote(g, j, r, c, 2 * n_rep + 1, {"fs": f + 1}))

    def start(copy):
        copy.start()

    def drain(copy):
        copy.wait_send()

    def onward(g, p, c, act):
        j = order(p)

        @pl.when(j > f)
        def _():
            along(g, j, c, 0, act)

        @pl.when(j < f)
        def _():
            along(g, j, c, 1, act)

        for d in range(1, n_rep):
            other = lax.rem(r + d, n_rep)
            act(remote(g, j, r, c, n_rep + other, {"rep": other}))

    def send_own(g):
        for c in range(chunk_counts[g]):
            along(g, f, c, 0, start)
            along(g, f, c, 1, start)

    def relay(g, p):
        for c in range(chunk_counts[g]):
            j = order(p)
            remote(g, j, r, c, 2 * n_rep, {"fs": f}).wait_recv()
            onward(g, p, c, start)

    def arrived(g, p):
        j = order(p)
        for d in range(1, n_rep):
            other = lax.rem(r + d, n_rep)
            for c in range(chunk_counts[g]):
                remote(g, j, other, c, n_rep + other, {"rep": other}).wait_recv()

    def block_of(index):
        return pl.ds(pl.multiple_of(index * rows, rows), rows)

    def tp_copies(kind, source, target):
        made = []
        for d in range(1, n_tp):
            other = lax.rem(t + d, n_tp)
            made.append(
                pltpu.make_async_remote_copy(
                    src_ref=source(other),
                    dst_ref=target(t),
                    send_sem=tp_send.at[kind, other],
                    recv_sem=tp_recv.at[kind, t],
                    device_id={"tp": other},
                    device_id_type=MESH,
                )
            )
        return made

    def tp_wait(kind, target):
        for d in range(1, n_tp):
            other = lax.rem(t + d, n_tp)
            pltpu.make_async_remote_copy(
                src_ref=target(other),
                dst_ref=target(other),
                send_sem=tp_send.at[kind, other],
                recv_sem=tp_recv.at[kind, other],
                device_id={"tp": other},
                device_id_type=MESH,
            ).wait_recv()

    stream = tokens[...].astype(jnp.float32)
    scale = lax.rsqrt(jnp.mean(stream * stream, axis=-1, keepdims=True) + epsilon)
    normed[block_of(t), :] = (stream * scale * gain1[...]).astype(jnp.bfloat16)

    pl.semaphore_wait(barrier, len(greeted))
    loads[0].wait()
    send_own(0)
    loads[1].wait()
    send_own(1)
    normed_at = lambda index: normed.at[block_of(index), :]
    sends = tp_copies(0, lambda other: normed_at(t), normed_at)
    for copy in sends:
        copy.start()
    for p in range(1, n_fs):
        relay(0, p)
        relay(1, p)
    loads[2].wait()
    send_own(2)

    tp_wait(0, normed_at)
    for p in range(1, n_fs):
        arrived(0, p)
    total = dot(normed[:, :part], in_buf[0])
    for index in range(1, n_fs):
        total += dot(normed[:, index * part : (index + 1) * part], in_buf[index])
    projected[...] = total.astype(jnp.bfloat16).astype(jnp.float32)
    groups, channels = group_weight.shape[0], group_weight.shape[1]
    position = lax.broadcasted_iota(jnp.int32, (length, channels), 0)
    for group in range(groups):
        lanes = slice(group * channels, (group + 1) * channels)
        values = projected[:, lanes]
        level_of = jnp.full((length, channels), lax.rem(t * groups + group, LEVELS), jnp.int32)
        running = values
        mean = jnp.zeros_like(values)
        for level in range(LEVELS):
            offset = 2**level
            running = running + jnp.where(position >= offset, pltpu.roll(running, offset, 0), 0.0)
            count = jnp.minimum(position + 1, 2 * offset).astype(jnp.float32)
            mean = jnp.where(level_of == level, running / count, mean)
        pooled = (mean - values).astype(jnp.bfloat16)
        mapped = dot(pooled, group_weight[group])
        pool_out[:, lanes] = (mapped * pool_scale[:, lanes]).astype(jnp.bfloat16)

    for p in range(1, n_fs):
        arrived(1, p)
    for index in range(n_fs):
        mix_send[index] = dot(pool_out[...], out_buf[index]).astype(jnp.bfloat16)
    more = tp_copies(
        1, lambda other: mix_send.at[:, block_of(other), :], lambda index: mix_recv.at[index]
    )
    relay(2, 1)
    for copy in more:
        copy.start()
    sends += more
    for p in range(2, n_fs - 1):
        relay(2, p)

    tp_wait(1, lambda index: mix_recv.at[index])
    square = jnp.zeros((rows, 1), jnp.float32)
    for index in range(n_fs):
        mixed = tokens[:, index * part : (index + 1) * part].astype(jnp.float32)
        mixed += mix_send[index, block_of(t), :].astype(jnp.float32)
        for d in range(1, n_tp):
            mixed += mix_recv[lax.rem(t + d, n_tp), index].astype(jnp.float32)
        stream2[index] = mixed
        square += jnp.sum(mixed * mixed, axis=-1, keepdims=True)
    scale = lax.rsqrt(square / width + epsilon)
    for index in range(n_fs):
        columns = slice(index * part, (index + 1) * part)
        normed2[block_of(t), columns] = (stream2[index] * scale * gain2[:, columns]).astype(
            jnp.bfloat16
        )
    normed2_at = lambda index: normed2.at[block_of(index), :]
    more = tp_copies(2, lambda other: normed2_at(t), normed2_at)
    for copy in more:
        copy.start()
    sends += more
    if n_fs > 2:
        relay(2, n_fs - 1)
    loads[3].wait()
    send_own(3)

    tp_wait(2, normed2_at)
    up_columns = up_buf.shape[2]
    up_tile = tile_of(up_columns, 512)

    def up_product(p):
        j = order(p)
        left = normed2.at[:, pl.ds(pl.multiple_of(j * part, part), part)]

        @pl.loop(0, up_columns // up_tile)
        def _(i):
            columns = pl.ds(pl.multiple_of(i * up_tile, up_tile), up_tile)
            product = dot(left[...], up_buf[j, :, columns])
            if p == 0:
                upper[:, columns] = product
            elif p < n_fs - 1:
                upper[:, columns] += product
            else:
                value = jnp.maximum(upper[:, columns] + product, 0.0)
                hidden[:, columns] = (value * value).astype(jnp.bfloat16)

    up_product(0)
    for p in range(1, n_fs):
        if p == n_fs - 1:
            relay(3, 1)
        arrived(2, p)
        up_product(p)

    down_tile = tile_of(part, 256)

    def sum_kind(p):
        return 3 + p

    def down_product(p):
        j = order(p)

        @pl.loop(0, part // down_tile)
        def _(i):
            columns = pl.ds(pl.multiple_of(i * down_tile, down_tile), down_tile)
            sum_send[p, :, columns] = dot(hidden[...], down_buf[j, :, columns]).astype(jnp.bfloat16)

        copies = tp_copies(
            sum_kind(p),
            lambda other: sum_send.at[p, block_of(other), :],
            lambda index: sum_recv.at[p, index],
        )
        for copy in copies:
            copy.start()
        return copies

    def finish(p):
        j = order(p)
        tp_wait(sum_kind(p), lambda index: sum_recv.at[p, index])
        channel = sum_send[p, block_of(t), :].astype(jnp.float32)
        for d in range(1, n_tp):
            channel += sum_recv[p, lax.rem(t + d, n_tp)].astype(jnp.float32)
        columns = pl.ds(pl.multiple_of(j * part, part), part)
        result[:, columns] = (stream2[j] + channel).astype(jnp.bfloat16)

    sends += down_product(0)
    for p in range(1, n_fs):
        if p < n_fs - 1:
            relay(3, p + 1)
        arrived(3, p)
        sends += down_product(p)
        finish(p - 1)
    for g in range(4):
        for c in range(chunk_counts[g]):
            along(g, f, c, 0, drain)
            along(g, f, c, 1, drain)
            for p in range(1, n_fs):
                onward(g, p, c, drain)
    finish(n_fs - 1)
    for copy in sends:
        copy.wait_send()


def local(sizes, tokens, gain1, in_w, group_w, pool_scale, out_w, gain2, up_w, down_w):
    n_rep, n_fs, n_tp = sizes
    rows, width = tokens.shape
    length, part = rows * n_tp, width // n_fs
    channels, hidden_units = in_w.shape[1], up_w.shape[1]
    bf16, f32 = jnp.bfloat16, jnp.float32
    weights = (in_w, out_w, up_w, down_w)
    vmem = pl.BlockSpec(memory_space=pltpu.VMEM)
    hbm = pl.BlockSpec(memory_space=pl.ANY)
    return pl.pallas_call(
        functools.partial(kernel, sizes),
        name="layer",
        out_shape=jax.ShapeDtypeStruct((rows, width), bf16),
        in_specs=[vmem, vmem, hbm, vmem, vmem, hbm, vmem, hbm, hbm],
        out_specs=vmem,
        scratch_shapes=[pltpu.VMEM((n_fs,) + w.shape, bf16) for w in weights]
        + [
            pltpu.VMEM((length, width), bf16),
            pltpu.VMEM((length, channels), f32),
            pltpu.VMEM((length, channels), bf16),
            pltpu.VMEM((n_fs, length, part), bf16),
            pltpu.VMEM((n_tp, n_fs, rows, part), bf16),
            pltpu.VMEM((n_fs, rows, part), f32),
            pltpu.VMEM((length, width), bf16),
            pltpu.VMEM((length, hidden_units), f32),
            pltpu.VMEM((length, hidden_units), bf16),
            pltpu.VMEM((n_fs, length, part), bf16),
            pltpu.VMEM((n_fs, n_tp, rows, part), bf16),
            pltpu.SemaphoreType.DMA((len(weights),)),
        ]
        + [
            pltpu.SemaphoreType.DMA((n_fs, 2 * n_rep + 2, chunks_of(*w.shape, n_rep)))
            for w in weights
        ]
        + [pltpu.SemaphoreType.DMA((3 + n_fs, n_tp))] * 2,
        compiler_params=pltpu.CompilerParams(
            collective_id=0, has_side_effects=True, vmem_limit_bytes=60 * 1024 * 1024
        ),
    )(
        tokens,
        gain1.reshape(1, -1),
        in_w,
        group_w,
        pool_scale.reshape(1, -1),
        out_w,
        gain2.reshape(1, -1),
        up_w,
        down_w,
    )


def solution(mesh):
    sizes = tuple(mesh.shape[axis] for axis in ("rep", "fs", "tp"))
    in_specs = (
        P(("rep", "fs", "tp"), None),
        P(),
        P("fs", "tp"),
        P("tp", None, None),
        P("tp"),
        P("tp", "fs"),
        P(),
        P("fs", "tp"),
        P("tp", "fs"),
    )
    return jax.shard_map(
        functools.partial(local, sizes),
        mesh=mesh,
        in_specs=in_specs,
        out_specs=P(("rep", "fs", "tp"), None),
        check_vma=False,
    )
```

profile of v0, /device:TPU:29, one launch (start us, length us, event | category | flops | bytes accessed | tf_op | source)
XLA Modules:
  0.0 185.6 jit_solution(13111315178949452569)
XLA Ops:
  0.0 183.8 %layer.1 = bf16[128,2048]{1,0:T(8,128)(2,1)} custom-call(bf16[128,2048]{1,0:T(8,128)(2,1)} %tokens.1, f32[1,2048]{1,0:T(1,128)} %bitcast.3, bf16[512,256]{1,0:T(8,128)(2,1)} %in_hbm.1, bf16[2,128,128]{2,1,0:T(8,128)(2,1)} %group_weight.1, f32[1,256]{1,0:T(1,128)} %bitcast.5, bf16[256,512]{1,0:T(8,128)(2,1)} %out_hbm.1, f32[1,2048]{1,0:T(1,128)} %bitcast.4, ...), custom_call_target="tpu_custom_call" | custom-call | tf_op jit(solution)/shard_map/layer/pallas_call | solution.py:373
  183.8 1.9 %copy.11 = bf16[128,2048]{1,0:T(8,128)(2,1)} copy(bf16[128,2048]{1,0:T(8,128)(2,1)} %layer.1) | data formatting | bytes 1048576
where the time goes:
time: 186 us
  Pallas kernels  184 us (99%)
  local copies, waits for them, and re-layouts  1.88 us (1%)
    pallas_call x1, Pallas kernels, local(): pl.pallas_call(functools.partial(kernel, sizes), name='layer', out_shape=...  184 us

commit v1 on v0

v1 whole, which is shorter than its diff:
```python
import functools

import jax
import jax.numpy as jnp
from jax import lax
from jax.experimental import pallas as pl
from jax.experimental.pallas import tpu as pltpu
from jax.sharding import PartitionSpec as P

MESH = pl.DeviceIdType.MESH
CHUNK_BYTES = 128 * 1024
SUB_COLUMNS = 256
LEVELS = 4

epsilon = 1e-06


def chunks_of(rows, columns, parts):
    count = max(1, rows * columns * 2 // parts // CHUNK_BYTES)
    while (rows // parts) % (count * 16):
        count -= 1
    return count


def dot(a, b):
    return jnp.dot(a, b, preferred_element_type=jnp.float32)


def tile_of(columns, most):
    tile = min(columns, most)
    while columns % tile:
        tile //= 2
    return tile


def kernel(
    sizes,
    tokens,
    gain1,
    in_hbm,
    group_weight,
    pool_scale,
    out_hbm,
    gain2,
    up_hbm,
    down_hbm,
    result,
    in_buf,
    out_buf,
    up_buf,
    down_buf,
    up_stage,
    down_stage,
    normed,
    projected,
    pool_out,
    mix_send,
    mix_recv,
    stream2,
    shared,
    hidden,
    core_send,
    core_recv,
    line_send,
    line_recv,
    pair_send,
    pair_recv,
    local_sem,
    in_sems,
    out_sems,
    up_sems,
    down_sems,
    tp_send,
    tp_recv,
    share_send,
    share_recv,
    core_sems,
    line_sems,
    pair_sems,
):
    n_rep, n_fs, n_tp = sizes
    n_y = n_tp // 2
    r, f, t = lax.axis_index("rep"), lax.axis_index("fs"), lax.axis_index("tp")
    core, y = lax.rem(t, 2), t // 2
    half = lax.rem(f, 2)
    f_pair, t_pair = f + 1 - 2 * half, t + 1 - 2 * core
    rows = tokens.shape[0]
    length = rows * n_tp
    width = tokens.shape[1]
    part = width // n_fs
    subs = down_buf.shape[1]
    sub_columns = down_buf.shape[3]
    steps = n_fs * subs
    half_units = up_buf.shape[3]
    gathered = ((in_buf, in_sems), (out_buf, out_sems))
    chunk_counts = [chunks_of(b.shape[1], b.shape[2], n_rep) for b, _ in gathered]
    spread = ((up_buf, up_stage, up_sems), (down_buf, down_stage, down_sems))
    spread_counts = [chunks_of(b.shape[2], b.shape[3], n_rep) for b, _, _ in spread]

    loads = []

    def load(source, target):
        copy = pltpu.make_async_copy(source, target, local_sem.at[len(loads)])
        copy.start()
        loads.append(copy)

    def units_of(which):
        return pl.ds(pl.multiple_of(which * half_units, half_units), half_units)

    load(in_hbm, in_buf.at[f])
    load(out_hbm, out_buf.at[f])
    load(up_hbm.at[:, units_of(1 - half)], up_stage.at[0])
    load(up_hbm.at[:, units_of(half)], up_buf.at[f, 0])
    for s in range(subs):
        columns = pl.ds(s * sub_columns, sub_columns)
        load(down_hbm.at[units_of(1 - half), columns], down_stage.at[s])
        load(down_hbm.at[units_of(half), columns], down_buf.at[f, s])

    barrier = pltpu.get_barrier_semaphore()
    greeted = [{"fs": lax.rem(f + d, n_fs)} for d in range(1, n_fs)]
    greeted += [{"rep": lax.rem(r + d, n_rep)} for d in range(1, n_rep)]
    greeted += [{"tp": lax.rem(t + d, n_tp)} for d in range(1, n_tp)]
    for device in greeted:
        pl.semaphore_signal(barrier, inc=1, device_id=device, device_id_type=MESH)

    def order(p):
        nearest = jnp.minimum(f, n_fs - 1 - f)
        step = (p + 1) // 2
        near = f + step if p % 2 else f - step
        far = f + (p - nearest) * jnp.where(2 * f < n_fs, 1, -1)
        return jnp.where(p <= 2 * nearest, near, far)

    def piece(g, j, q, c):
        buf = gathered[g][0]
        size = buf.shape[1] // n_rep // chunk_counts[g]
        start = pl.multiple_of((q * chunk_counts[g] + c) * size, size)
        return buf.at[j, pl.ds(start, size), :]

    def remote(g, j, q, c, send_slot, device):
        block = piece(g, j, q, c)
        sems = gathered[g][1]
        return pltpu.make_async_remote_copy(
            src_ref=block,
            dst_ref=block,
            send_sem=sems.at[j, send_slot, c],
            recv_sem=sems.at[j, q, c],
            device_id=device,
            device_id_type=MESH,
        )

    def along(g, j, c, way, act):
        if way == 0:

            @pl.when(f > 0)
            def _():
                act(remote(g, j, r, c, 2 * n_rep, {"fs": f - 1}))

        else:

            @pl.when(f < n_fs - 1)
            def _():
                act(remote(g, j, r, c, 2 * n_rep + 1, {"fs": f + 1}))

    def start(copy):
        copy.start()

    def drain(copy):
        copy.wait_send()

    def onward(g, p, c, act):
        j = order(p)

        @pl.when(j > f)
        def _():
            along(g, j, c, 0, act)

        @pl.when(j < f)
        def _():
            along(g, j, c, 1, act)

        for d in range(1, n_rep):
            other = lax.rem(r + d, n_rep)
            act(remote(g, j, r, c, n_rep + other, {"rep": other}))

    def send_own(g):
        for c in range(chunk_counts[g]):
            along(g, f, c, 0, start)
            along(g, f, c, 1, start)

    def relay(g, p):
        for c in range(chunk_counts[g]):
            j = order(p)
            remote(g, j, r, c, 2 * n_rep, {"fs": f}).wait_recv()
            onward(g, p, c, start)

    def arrived(g, p):
        j = order(p)
        for d in range(1, n_rep):
            other = lax.rem(r + d, n_rep)
            for c in range(chunk_counts[g]):
                remote(g, j, other, c, n_rep + other, {"rep": other}).wait_recv()

    def block_of(index):
        return pl.ds(pl.multiple_of(index * rows, rows), rows)

    def copy_to(source, target, send_sem, recv_sem, device):
        return pltpu.make_async_remote_copy(
            src_ref=source,
            dst_ref=target,
            send_sem=send_sem,
            recv_sem=recv_sem,
            device_id=device,
            device_id_type=MESH,
        )

    def tp_copies(kind, source, target):
        made = []
        for d in range(1, n_tp):
            other = lax.rem(t + d, n_tp)
            made.append(
                copy_to(
                    source(other),
                    target(t),
                    tp_send.at[kind, other],
                    tp_recv.at[kind, t],
                    {"tp": other},
                )
            )
        return made

    def tp_wait(kind, target):
        for d in range(1, n_tp):
            other = lax.rem(t + d, n_tp)
            copy_to(
                target(other),
                target(other),
                tp_send.at[kind, other],
                tp_recv.at[kind, other],
                {"tp": other},
            ).wait_recv()

    sends = []

    def send(copy):
        copy.start()
        sends.append(copy)

    def spread_rows(g, q, c):
        size = spread[g][0].shape[2] // n_rep // spread_counts[g]
        return pl.ds(pl.multiple_of((q * spread_counts[g] + c) * size, size), size)

    def source_of(d):
        return lax.rem(f - d + n_fs, n_fs)

    def spread_own(g, d):
        buf, stage, sems = spread[g]
        to = lax.rem(f + d, n_fs)
        for s in range(buf.shape[1]):
            for c in range(spread_counts[g]):
                piece = spread_rows(g, r, c)
                target = buf.at[f, s, piece, :]
                source = stage.at[s, piece, :] if d % 2 else target
                send(copy_to(source, target, sems.at[0, to, s, c], sems.at[1, f, s, c], {"fs": to}))

    def spread_relay(g, d, s):
        buf, _, sems = spread[g]
        j = source_of(d)
        for c in range(spread_counts[g]):
            block = buf.at[j, s, spread_rows(g, r, c), :]
            copy_to(block, block, sems.at[0, j, s, c], sems.at[1, j, s, c], {"fs": j}).wait_recv()
            for e in range(1, n_rep):
                other = lax.rem(r + e, n_rep)
                send(
                    copy_to(
                        block,
                        block,
                        sems.at[2 + other, j, s, c],
                        sems.at[2 + n_rep + r, j, s, c],
                        {"rep": other},
                    )
                )

    def spread_arrived(g, d, s):
        buf, _, sems = spread[g]
        j = source_of(d)
        for e in range(1, n_rep):
            other = lax.rem(r + e, n_rep)
            for c in range(spread_counts[g]):
                block = buf.at[j, s, spread_rows(g, other, c), :]
                copy_to(
                    block,
                    block,
                    sems.at[2 + other, j, s, c],
                    sems.at[2 + n_rep + other, j, s, c],
                    {"rep": other},
                ).wait_recv()

    stream = tokens[...].astype(jnp.float32)
    scale = lax.rsqrt(jnp.mean(stream * stream, axis=-1, keepdims=True) + epsilon)
    normed[block_of(t), :] = (stream * scale * gain1[...]).astype(jnp.bfloat16)

    pl.semaphore_wait(barrier, len(greeted))
    loads[0].wait()
    send_own(0)
    loads[1].wait()
    send_own(1)
    normed_at = lambda index: normed.at[block_of(index), :]
    for copy in tp_copies(0, lambda other: normed_at(t), normed_at):
        send(copy)
    for p in range(1, n_fs):
        relay(0, p)
        relay(1, p)
    loads[2].wait()
    loads[3].wait()
    for d in range(1, n_fs):
        spread_own(0, d)
    for copy in loads[4:]:
        copy.wait()
    spread_own(1, 1)

    tp_wait(0, normed_at)
    for p in range(1, n_fs):
        arrived(0, p)
    total = dot(normed[:, :part], in_buf[0])
    for index in range(1, n_fs):
        total += dot(normed[:, index * part : (index + 1) * part], in_buf[index])
    projected[...] = total.astype(jnp.bfloat16).astype(jnp.float32)
    groups, channels = group_weight.shape[0], group_weight.shape[1]
    position = lax.broadcasted_iota(jnp.int32, (length, channels), 0)
    for group in range(groups):
        lanes = slice(group * channels, (group + 1) * channels)
        values = projected[:, lanes]
        level_of = jnp.full((length, channels), lax.rem(t * groups + group, LEVELS), jnp.int32)
        running = values
        mean = jnp.zeros_like(values)
        for level in range(LEVELS):
            offset = 2**level
            running = running + jnp.where(position >= offset, pltpu.roll(running, offset, 0), 0.0)
            count = jnp.minimum(position + 1, 2 * offset).astype(jnp.float32)
            mean = jnp.where(level_of == level, running / count, mean)
        pooled = (mean - values).astype(jnp.bfloat16)
        mapped = dot(pooled, group_weight[group])
        pool_out[:, lanes] = (mapped * pool_scale[:, lanes]).astype(jnp.bfloat16)

    for p in range(1, n_fs):
        arrived(1, p)
    for index in range(n_fs):
        mix_send[index] = dot(pool_out[...], out_buf[index]).astype(jnp.bfloat16)
    for copy in tp_copies(
        1, lambda other: mix_send.at[:, block_of(other), :], lambda index: mix_recv.at[index]
    ):
        send(copy)
    for d in range(1, n_fs - 1):
        spread_relay(0, d, 0)

    tp_wait(1, lambda index: mix_recv.at[index])
    square = jnp.zeros((rows, 1), jnp.float32)
    for index in range(n_fs):
        mixed = tokens[:, index * part : (index + 1) * part].astype(jnp.float32)
        mixed += mix_send[index, block_of(t), :].astype(jnp.float32)
        for d in range(1, n_tp):
            mixed += mix_recv[lax.rem(t + d, n_tp), index].astype(jnp.float32)
        stream2[index] = mixed
        square += jnp.sum(mixed * mixed, axis=-1, keepdims=True)
    scale = lax.rsqrt(square / width + epsilon)

    def place_of(owner):
        return block_of(lax.rem(owner, 2) * n_y + owner // 2)

    for index in range(n_fs):
        columns = slice(index * part, (index + 1) * part)
        shared[half, place_of(t), columns] = (stream2[index] * scale * gain2[:, columns]).astype(
            jnp.bfloat16
        )

    def share(plane, owner, send_slot, device):
        block = shared.at[plane, place_of(owner), :]
        return copy_to(
            block, block, share_send.at[send_slot, plane, owner], share_recv.at[plane, owner], device
        )

    def share_core(plane, owner):
        send(share(plane, owner, n_y, {"tp": t_pair}))

    def on_line(e):
        return lax.rem(y + e, n_y)

    def share_line(plane):
        for e in range(1, n_y):
            to = on_line(e)
            send(share(plane, t, to, {"tp": 2 * to + core}))

    def shared_from(plane, owner):
        share(plane, owner, n_y, {"tp": t_pair}).wait_recv()

    def shared_by_core(plane):
        for e in range(n_y):
            shared_from(plane, 2 * on_line(e) + 1 - core)

    send(share(half, t, n_y + 1, {"fs": f_pair}))
    share_line(half)
    share_core(half, t)
    for d in range(2, n_fs):
        spread_own(1, d)
    spread_relay(0, n_fs - 1, 0)
    for e in range(1, n_y):
        owner = 2 * on_line(e) + core
        shared_from(half, owner)
        share_core(half, owner)
    shared_from(1 - half, t)
    share_line(1 - half)
    share_core(1 - half, t)
    shared_by_core(half)
    for d in range(1, n_fs):
        spread_arrived(0, d, 0)

    up_tile = tile_of(half_units, 256)

    def up_product(plane):
        @pl.loop(0, half_units // up_tile)
        def _(i):
            columns = pl.ds(pl.multiple_of(i * up_tile, up_tile), up_tile)
            total = dot(shared[plane, :, :part], up_buf[0, 0, :, columns])
            for index in range(1, n_fs):
                left = shared[plane, :, index * part : (index + 1) * part]
                total += dot(left, up_buf[index, 0, :, columns])
            value = jnp.maximum(total, 0.0)
            hidden[plane, :, columns] = (value * value).astype(jnp.bfloat16)

    up_product(half)
    for s in range(subs):
        spread_relay(1, 1, s)
    for e in range(1, n_y):
        owner = 2 * on_line(e) + core
        shared_from(1 - half, owner)
        share_core(1 - half, owner)
    shared_by_core(1 - half)
    up_product(1 - half)

    line_rows = n_y * rows

    def own_rows(which):
        return pl.ds(pl.multiple_of(which * line_rows, line_rows), line_rows)

    def down_product(k):
        d, s = k // subs, k % subs
        j = source_of(d)
        if d:
            spread_arrived(1, d, s)
        for plane in range(2):
            product = dot(hidden[plane], down_buf[j, s])
            core_send[k, plane] = product.astype(jnp.bfloat16)
        send(
            copy_to(
                core_send.at[k, :, own_rows(1 - core), :],
                core_recv.at[k],
                core_sems.at[0, k],
                core_sems.at[1, k],
                {"tp": t_pair},
            )
        )

    def to_line(k):
        copy_to(
            core_recv.at[k], core_recv.at[k], core_sems.at[0, k], core_sems.at[1, k], {"tp": t_pair}
        ).wait_recv()
        for plane in range(2):
            own = core_send[k, plane, own_rows(core), :].astype(jnp.float32)
            both = own + core_recv[k, plane].astype(jnp.float32)
            line_send[k, plane] = both.astype(jnp.bfloat16)
        for e in range(1, n_y):
            to = on_line(e)
            send(
                copy_to(
                    line_send.at[k, :, block_of(to), :],
                    line_recv.at[k, y],
                    line_sems.at[0, k, to],
                    line_sems.at[1, k, y],
                    {"tp": 2 * to + core},
                )
            )

    def to_pair(k):
        d, s = k // subs, k % subs
        j = source_of(d)
        for e in range(1, n_y):
            block = line_recv.at[k, on_line(e)]
            copy_to(
                block,
                block,
                line_sems.at[0, k, on_line(e)],
                line_sems.at[1, k, on_line(e)],
                {"tp": t_pair},
            ).wait_recv()

        def total_of(plane):
            total = core_send[k, plane, block_of(core * n_y + y), :].astype(jnp.float32)
            total += core_recv[k, plane, block_of(y), :].astype(jnp.float32)
            for e in range(1, n_y):
                total += line_recv[k, on_line(e), plane].astype(jnp.float32)
            return total

        pair_send[j * subs + s] = total_of(1 - half).astype(jnp.bfloat16)
        send(
            copy_to(
                pair_send.at[j * subs + s],
                pair_recv.at[j * subs + s],
                pair_sems.at[0, j * subs + s],
                pair_sems.at[1, j * subs + s],
                {"fs": f_pair},
            )
        )
        columns = slice(s * sub_columns, (s + 1) * sub_columns)
        stream2[j, :, columns] += total_of(half)

    def finish(k):
        d, s = k // subs, k % subs
        j = lax.rem(f - half - d + n_fs, n_fs)
        slot = j * subs + s
        copy_to(
            pair_recv.at[slot],
            pair_recv.at[slot],
            pair_sems.at[0, slot],
            pair_sems.at[1, slot],
            {"fs": f_pair},
        ).wait_recv()
        columns = slice(s * sub_columns, (s + 1) * sub_columns)
        value = stream2[j, :, columns] + pair_recv[slot].astype(jnp.float32)
        target = pl.ds(pl.multiple_of(j * part + s * sub_columns, sub_columns), sub_columns)
        result[:, target] = value.astype(jnp.bfloat16)

    for k in range(steps + 3 + subs):
        if 2 * subs <= k + 1 < steps:
            spread_relay(1, (k + 1) // subs, (k + 1) % subs)
        if k < steps:
            down_product(k)
        if 0 <= k - 1 < steps:
            to_line(k - 1)
        if 0 <= k - 2 < steps:
            to_pair(k - 2)
        if 0 <= k - 3 - subs < steps:
            finish(k - 3 - subs)

    for g in range(2):
        for c in range(chunk_counts[g]):
            along(g, f, c, 0, drain)
            along(g, f, c, 1, drain)
            for p in range(1, n_fs):
                onward(g, p, c, drain)
    for copy in sends:
        copy.wait_send()


def local(sizes, tokens, gain1, in_w, group_w, pool_scale, out_w, gain2, up_w, down_w):
    n_rep, n_fs, n_tp = sizes
    n_y = n_tp // 2
    rows, width = tokens.shape
    length, part = rows * n_tp, width // n_fs
    channels, half_units = in_w.shape[1], up_w.shape[1] // 2
    sub_columns = tile_of(part, SUB_COLUMNS)
    subs = part // sub_columns
    steps = n_fs * subs
    bf16, f32 = jnp.bfloat16, jnp.float32
    vmem = pl.BlockSpec(memory_space=pltpu.VMEM)
    hbm = pl.BlockSpec(memory_space=pl.ANY)
    dma = pltpu.SemaphoreType.DMA
    kinds = 2 + 2 * n_rep
    return pl.pallas_call(
        functools.partial(kernel, sizes),
        name="layer",
        out_shape=jax.ShapeDtypeStruct((rows, width), bf16),
        in_specs=[vmem, vmem, hbm, vmem, vmem, hbm, vmem, hbm, hbm],
        out_specs=vmem,
        scratch_shapes=[
            pltpu.VMEM((n_fs,) + in_w.shape, bf16),
            pltpu.VMEM((n_fs,) + out_w.shape, bf16),
            pltpu.VMEM((n_fs, 1, part, half_units), bf16),
            pltpu.VMEM((n_fs, subs, half_units, sub_columns), bf16),
            pltpu.VMEM((1, part, half_units), bf16),
            pltpu.VMEM((subs, half_units, sub_columns), bf16),
            pltpu.VMEM((length, width), bf16),
            pltpu.VMEM((length, channels), f32),
            pltpu.VMEM((length, channels), bf16),
            pltpu.VMEM((n_fs, length, part), bf16),
            pltpu.VMEM((n_tp, n_fs, rows, part), bf16),
            pltpu.VMEM((n_fs, rows, part), f32),
            pltpu.VMEM((2, length, width), bf16),
            pltpu.VMEM((2, length, half_units), bf16),
            pltpu.VMEM((steps, 2, length, sub_columns), bf16),
            pltpu.VMEM((steps, 2, n_y * rows, sub_columns), bf16),
            pltpu.VMEM((steps, 2, n_y * rows, sub_columns), bf16),
            pltpu.VMEM((steps, n_y, 2, rows, sub_columns), bf16),
            pltpu.VMEM((steps, rows, sub_columns), bf16),
            pltpu.VMEM((steps, rows, sub_columns), bf16),
            dma((4 + 2 * subs,)),
            dma((n_fs, 2 * n_rep + 2, chunks_of(*in_w.shape, n_rep))),
            dma((n_fs, 2 * n_rep + 2, chunks_of(*out_w.shape, n_rep))),
            dma((kinds, n_fs, 1, chunks_of(part, half_units, n_rep))),
            dma((kinds, n_fs, subs, chunks_of(half_units, sub_columns, n_rep))),
            dma((2, n_tp)),
            dma((2, n_tp)),
            dma((n_y + 2, 2, n_tp)),
            dma((2, n_tp)),
            dma((2, steps)),
            dma((2, steps, n_y)),
            dma((2, steps)),
        ],
        compiler_params=pltpu.CompilerParams(
            collective_id=0, has_side_effects=True, vmem_limit_bytes=60 * 1024 * 1024
        ),
    )(
        tokens,
        gain1.reshape(1, -1),
        in_w,
        group_w,
        pool_scale.reshape(1, -1),
        out_w,
        gain2.reshape(1, -1),
        up_w,
        down_w,
    )


def solution(mesh):
    sizes = tuple(mesh.shape[axis] for axis in ("rep", "fs", "tp"))
    in_specs = (
        P(("rep", "fs", "tp"), None),
        P(),
        P("fs", "tp"),
        P("tp", None, None),
        P("tp"),
        P("tp", "fs"),
        P(),
        P("fs", "tp"),
        P("tp", "fs"),
    )
    return jax.shard_map(
        functools.partial(local, sizes),
        mesh=mesh,
        in_specs=in_specs,
        out_specs=P(("rep", "fs", "tp"), None),
        check_vma=False,
    )
```

time: 186 us -> 164 us (0.88)
  the two profiles are of different devices: /device:TPU:29 before, /device:TPU:0 now
where the time goes in v1:
time: 164 us
  Pallas kernels  162 us (99%)
  local copies, waits for them, and re-layouts  1.88 us (1%)
    pallas_call x1, Pallas kernels, local(): pl.pallas_call(functools.partial(kernel, sizes), name='layer', out_shape=...  162 us

profile of v1, /device:TPU:0, one launch (start us, length us, event | category | flops | bytes accessed | tf_op | source)
XLA Modules:
  0.0 163.7 jit_solution(1167242928140366574)
XLA Ops:
  0.0 161.8 %layer.1 = bf16[128,2048]{1,0:T(8,128)(2,1)} custom-call(bf16[128,2048]{1,0:T(8,128)(2,1)} %tokens.1, f32[1,2048]{1,0:T(1,128)} %bitcast.3, bf16[512,256]{1,0:T(8,128)(2,1)} %in_hbm.1, bf16[2,128,128]{2,1,0:T(8,128)(2,1)} %group_weight.1, f32[1,256]{1,0:T(1,128)} %bitcast.5, bf16[256,512]{1,0:T(8,128)(2,1)} %out_hbm.1, f32[1,2048]{1,0:T(1,128)} %bitcast.4, ...), custom_call_target="tpu_custom_call" | custom-call | tf_op jit(solution)/shard_map/layer/pallas_call | solution.py:568
  161.8 1.9 %copy.11 = bf16[128,2048]{1,0:T(8,128)(2,1)} copy(bf16[128,2048]{1,0:T(8,128)(2,1)} %layer.1) | data formatting | bytes 1048576

commit v2 on v1

--- a/solution.py
+++ b/solution.py
@@ -10,6 +10,7 @@
 MESH = pl.DeviceIdType.MESH
 CHUNK_BYTES = 128 * 1024
 SUB_COLUMNS = 256
+SHARE_CHUNKS = 4
 LEVELS = 4
 
 epsilon = 1e-06
@@ -49,13 +50,13 @@
     out_buf,
     up_buf,
     down_buf,
-    up_stage,
-    down_stage,
     normed,
     projected,
     pool_out,
     mix_send,
-    mix_recv,
+    mix_core,
+    mix_line_send,
+    mix_line,
     stream2,
     shared,
     hidden,
@@ -70,8 +71,10 @@
     out_sems,
     up_sems,
     down_sems,
-    tp_send,
-    tp_recv,
+    normed_send,
+    normed_recv,
+    mix_core_sems,
+    mix_line_sems,
     share_send,
     share_recv,
     core_sems,
@@ -94,8 +97,8 @@
     half_units = up_buf.shape[3]
     gathered = ((in_buf, in_sems), (out_buf, out_sems))
     chunk_counts = [chunks_of(b.shape[1], b.shape[2], n_rep) for b, _ in gathered]
-    spread = ((up_buf, up_stage, up_sems), (down_buf, down_stage, down_sems))
-    spread_counts = [chunks_of(b.shape[2], b.shape[3], n_rep) for b, _, _ in spread]
+    spread = ((up_buf, up_sems), (down_buf, down_sems))
+    spread_counts = [chunks_of(b.shape[2], b.shape[3], n_rep) for b, _ in spread]
 
     loads = []
 
@@ -109,11 +112,11 @@
 
     load(in_hbm, in_buf.at[f])
     load(out_hbm, out_buf.at[f])
-    load(up_hbm.at[:, units_of(1 - half)], up_stage.at[0])
+    load(up_hbm.at[:, units_of(1 - half)], up_buf.at[n_fs, 0])
     load(up_hbm.at[:, units_of(half)], up_buf.at[f, 0])
     for s in range(subs):
         columns = pl.ds(s * sub_columns, sub_columns)
-        load(down_hbm.at[units_of(1 - half), columns], down_stage.at[s])
+        load(down_hbm.at[units_of(1 - half), columns], down_buf.at[n_fs, s])
         load(down_hbm.at[units_of(half), columns], down_buf.at[f, s])
 
     barrier = pltpu.get_barrier_semaphore()
@@ -123,11 +126,13 @@
     for device in greeted:
         pl.semaphore_signal(barrier, inc=1, device_id=device, device_id_type=MESH)
 
+    inward = jnp.where(2 * f < n_fs, 1, -1)
+
     def order(p):
         nearest = jnp.minimum(f, n_fs - 1 - f)
         step = (p + 1) // 2
-        near = f + step if p % 2 else f - step
-        far = f + (p - nearest) * jnp.where(2 * f < n_fs, 1, -1)
+        near = f + step * inward if p % 2 else f - step * inward
+        far = f + (p - nearest) * inward
         return jnp.where(p <= 2 * nearest, near, far)
 
     def piece(g, j, q, c):
@@ -213,32 +218,6 @@
             device_id_type=MESH,
         )
 
-    def tp_copies(kind, source, target):
-        made = []
-        for d in range(1, n_tp):
-            other = lax.rem(t + d, n_tp)
-            made.append(
-                copy_to(
-                    source(other),
-                    target(t),
-                    tp_send.at[kind, other],
-                    tp_recv.at[kind, t],
-                    {"tp": other},
-                )
-            )
-        return made
-
-    def tp_wait(kind, target):
-        for d in range(1, n_tp):
-            other = lax.rem(t + d, n_tp)
-            copy_to(
-                target(other),
-                target(other),
-                tp_send.at[kind, other],
-                tp_recv.at[kind, other],
-                {"tp": other},
-            ).wait_recv()
-
     sends = []
 
     def send(copy):
@@ -249,22 +228,39 @@
         size = spread[g][0].shape[2] // n_rep // spread_counts[g]
         return pl.ds(pl.multiple_of((q * spread_counts[g] + c) * size, size), size)
 
-    def source_of(d):
-        return lax.rem(f - d + n_fs, n_fs)
-
-    def spread_own(g, d):
-        buf, stage, sems = spread[g]
-        to = lax.rem(f + d, n_fs)
-        for s in range(buf.shape[1]):
-            for c in range(spread_counts[g]):
-                piece = spread_rows(g, r, c)
-                target = buf.at[f, s, piece, :]
-                source = stage.at[s, piece, :] if d % 2 else target
-                send(copy_to(source, target, sems.at[0, to, s, c], sems.at[1, f, s, c], {"fs": to}))
-
-    def spread_relay(g, d, s):
-        buf, _, sems = spread[g]
-        j = source_of(d)
+    farthest = list(range(n_fs - 1, 0, -1))
+    at_end = jnp.logical_or(f == 0, f == n_fs - 1)
+
+    def by_place(ends, k):
+        return jnp.where(at_end, order(ends[k - 1]), order(farthest[k - 1]))
+
+    def ranked(k):
+        return by_place([1] + farthest[:-1], k) if k else f
+
+    def sent(k):
+        return by_place(farthest[1:2] + farthest[:1] + farthest[2:], k)
+
+    def spread_own(g, act):
+        buf, sems = spread[g]
+        for k in range(1, n_fs):
+            to = sent(k)
+            slot = jnp.where(lax.rem(to, 2) == half, f, n_fs)
+            for s in range(buf.shape[1]):
+                for c in range(spread_counts[g]):
+                    piece = spread_rows(g, r, c)
+                    act(
+                        copy_to(
+                            buf.at[slot, s, piece, :],
+                            buf.at[f, s, piece, :],
+                            sems.at[0, to, s, c],
+                            sems.at[1, f, s, c],
+                            {"fs": to},
+                        )
+                    )
+
+    def spread_relay(g, k, s):
+        buf, sems = spread[g]
+        j = ranked(k)
         for c in range(spread_counts[g]):
             block = buf.at[j, s, spread_rows(g, r, c), :]
             copy_to(block, block, sems.at[0, j, s, c], sems.at[1, j, s, c], {"fs": j}).wait_recv()
@@ -280,9 +276,9 @@
                     )
                 )
 
-    def spread_arrived(g, d, s):
-        buf, _, sems = spread[g]
-        j = source_of(d)
+    def spread_arrived(g, k, s):
+        buf, sems = spread[g]
+        j = ranked(k)
         for e in range(1, n_rep):
             other = lax.rem(r + e, n_rep)
             for c in range(spread_counts[g]):
@@ -299,28 +295,44 @@
     scale = lax.rsqrt(jnp.mean(stream * stream, axis=-1, keepdims=True) + epsilon)
     normed[block_of(t), :] = (stream * scale * gain1[...]).astype(jnp.bfloat16)
 
+    def on_line(e):
+        return lax.rem(y + e, n_y)
+
+    def give_normed(owner, slot, device):
+        block = normed.at[block_of(owner), :]
+        return copy_to(block, block, normed_send.at[slot, owner], normed_recv.at[owner], device)
+
+    def normed_from(owner):
+        give_normed(owner, n_y, {"tp": t_pair}).wait_recv()
+
     pl.semaphore_wait(barrier, len(greeted))
+    for e in range(1, n_y):
+        to = on_line(e)
+        send(give_normed(t, to, {"tp": 2 * to + core}))
+    send(give_normed(t, n_y, {"tp": t_pair}))
     loads[0].wait()
     send_own(0)
     loads[1].wait()
     send_own(1)
-    normed_at = lambda index: normed.at[block_of(index), :]
-    for copy in tp_copies(0, lambda other: normed_at(t), normed_at):
-        send(copy)
     for p in range(1, n_fs):
         relay(0, p)
+    for p in range(1, n_fs):
         relay(1, p)
-    loads[2].wait()
-    loads[3].wait()
-    for d in range(1, n_fs):
-        spread_own(0, d)
-    for copy in loads[4:]:
+    for e in range(1, n_y):
+        owner = 2 * on_line(e) + core
+        normed_from(owner)
+        send(give_normed(owner, n_y, {"tp": t_pair}))
+    for copy in loads[2:]:
         copy.wait()
-    spread_own(1, 1)
-
-    tp_wait(0, normed_at)
+
+    @pl.when(at_end)
+    def _():
+        spread_own(0, start)
+
     for p in range(1, n_fs):
         arrived(0, p)
+    for e in range(n_y):
+        normed_from(2 * on_line(e) + 1 - core)
     total = dot(normed[:, :part], in_buf[0])
     for index in range(1, n_fs):
         total += dot(normed[:, index * part : (index + 1) * part], in_buf[index])
@@ -342,24 +354,57 @@
         mapped = dot(pooled, group_weight[group])
         pool_out[:, lanes] = (mapped * pool_scale[:, lanes]).astype(jnp.bfloat16)
 
+
+    @pl.when(jnp.logical_not(at_end))
+    def _():
+        spread_own(0, start)
+
     for p in range(1, n_fs):
         arrived(1, p)
+    def mix_by_core(index, e):
+        block = mix_send.at[index, block_of(2 * e + 1 - core), :]
+        sems = mix_core_sems
+        return copy_to(
+            block, mix_core.at[index, e], sems.at[0, index, e], sems.at[1, index, e], {"tp": t_pair}
+        )
+
+    def mix_by_line(index, source, target, to):
+        sems = mix_line_sems
+        return copy_to(
+            source, target, sems.at[0, index, to], sems.at[1, index, y], {"tp": 2 * to + core}
+        )
+
+    def mix_pair(index, which):
+        own = mix_send[index, block_of(2 * which + core), :].astype(jnp.float32)
+        return own + mix_core[index, which].astype(jnp.float32)
+
     for index in range(n_fs):
         mix_send[index] = dot(pool_out[...], out_buf[index]).astype(jnp.bfloat16)
-    for copy in tp_copies(
-        1, lambda other: mix_send.at[:, block_of(other), :], lambda index: mix_recv.at[index]
-    ):
-        send(copy)
-    for d in range(1, n_fs - 1):
-        spread_relay(0, d, 0)
-
-    tp_wait(1, lambda index: mix_recv.at[index])
+        for e in range(n_y):
+            send(mix_by_core(index, e))
+    for index in range(n_fs):
+        for e in range(n_y):
+            mix_by_core(index, e).wait_recv()
+        for e in range(1, n_y):
+            to = on_line(e)
+            mix_line_send[index, to] = mix_pair(index, to).astype(jnp.bfloat16)
+            send(mix_by_line(index, mix_line_send.at[index, to], mix_line.at[index, y], to))
+
+    spread_relay(0, 1, 0)
     square = jnp.zeros((rows, 1), jnp.float32)
     for index in range(n_fs):
         mixed = tokens[:, index * part : (index + 1) * part].astype(jnp.float32)
-        mixed += mix_send[index, block_of(t), :].astype(jnp.float32)
-        for d in range(1, n_tp):
-            mixed += mix_recv[lax.rem(t + d, n_tp), index].astype(jnp.float32)
+        mixed += mix_pair(index, y)
+        for e in range(1, n_y):
+            block = mix_line.at[index, on_line(e)]
+            copy_to(
+                block,
+                block,
+                mix_line_sems.at[0, index, on_line(e)],
+                mix_line_sems.at[1, index, on_line(e)],
+                {"tp": t_pair},
+            ).wait_recv()
+            mixed += block[...].astype(jnp.float32)
         stream2[index] = mixed
         square += jnp.sum(mixed * mixed, axis=-1, keepdims=True)
     scale = lax.rsqrt(square / width + epsilon)
@@ -373,44 +418,59 @@
             jnp.bfloat16
         )
 
-    def share(plane, owner, send_slot, device):
-        block = shared.at[plane, place_of(owner), :]
+    def share(plane, owner, c, send_slot, device):
+        size = rows // SHARE_CHUNKS
+        place = lax.rem(owner, 2) * n_y + owner // 2
+        start = pl.multiple_of(place * rows + c * size, size)
+        block = shared.at[plane, pl.ds(start, size), :]
         return copy_to(
-            block, block, share_send.at[send_slot, plane, owner], share_recv.at[plane, owner], device
+            block,
+            block,
+            share_send.at[send_slot, plane, owner, c],
+            share_recv.at[plane, owner, c],
+            device,
         )
 
-    def share_core(plane, owner):
-        send(share(plane, owner, n_y, {"tp": t_pair}))
-
-    def on_line(e):
-        return lax.rem(y + e, n_y)
-
-    def share_line(plane):
+    def share_core(plane, owner, c):
+        send(share(plane, owner, c, n_y, {"tp": t_pair}))
+
+    def share_line(plane, c):
         for e in range(1, n_y):
             to = on_line(e)
-            send(share(plane, t, to, {"tp": 2 * to + core}))
-
-    def shared_from(plane, owner):
-        share(plane, owner, n_y, {"tp": t_pair}).wait_recv()
+            send(share(plane, t, c, to, {"tp": 2 * to + core}))
+
+    def shared_from(plane, owner, c):
+        share(plane, owner, c, n_y, {"tp": t_pair}).wait_recv()
 
     def shared_by_core(plane):
         for e in range(n_y):
-            shared_from(plane, 2 * on_line(e) + 1 - core)
-
-    send(share(half, t, n_y + 1, {"fs": f_pair}))
-    share_line(half)
-    share_core(half, t)
-    for d in range(2, n_fs):
-        spread_own(1, d)
+            for c in range(SHARE_CHUNKS):
+                shared_from(plane, 2 * on_line(e) + 1 - core, c)
+
+    for c in range(SHARE_CHUNKS):
+        send(share(half, t, c, n_y + 1, {"fs": f_pair}))
+        share_line(half, c)
+        share_core(half, t, c)
+    spread_own(1, start)
+    for c in range(SHARE_CHUNKS):
+        for e in range(1, n_y):
+            owner = 2 * on_line(e) + core
+            shared_from(half, owner, c)
+            share_core(half, owner, c)
+    for k in range(2, n_fs - 1):
+        spread_relay(0, k, 0)
+    for c in range(SHARE_CHUNKS):
+        shared_from(1 - half, t, c)
+        share_line(1 - half, c)
+        share_core(1 - half, t, c)
     spread_relay(0, n_fs - 1, 0)
-    for e in range(1, n_y):
-        owner = 2 * on_line(e) + core
-        shared_from(half, owner)
-        share_core(half, owner)
-    shared_from(1 - half, t)
-    share_line(1 - half)
-    share_core(1 - half, t)
+    for c in range(SHARE_CHUNKS):
+        for e in range(1, n_y):
+            owner = 2 * on_line(e) + core
+            shared_from(1 - half, owner, c)
+            share_core(1 - half, owner, c)
     shared_by_core(half)
+    spread_relay(1, 1, 0)
     for d in range(1, n_fs):
         spread_arrived(0, d, 0)
 
@@ -428,12 +488,8 @@
             hidden[plane, :, columns] = (value * value).astype(jnp.bfloat16)
 
     up_product(half)
-    for s in range(subs):
+    for s in range(1, subs):
         spread_relay(1, 1, s)
-    for e in range(1, n_y):
-        owner = 2 * on_line(e) + core
-        shared_from(1 - half, owner)
-        share_core(1 - half, owner)
     shared_by_core(1 - half)
     up_product(1 - half)
 
@@ -444,7 +500,7 @@
 
     def down_product(k):
         d, s = k // subs, k % subs
-        j = source_of(d)
+        j = ranked(d)
         if d:
             spread_arrived(1, d, s)
         for plane in range(2):
@@ -482,7 +538,7 @@
 
     def to_pair(k):
         d, s = k // subs, k % subs
-        j = source_of(d)
+        j = ranked(d)
         for e in range(1, n_y):
             block = line_recv.at[k, on_line(e)]
             copy_to(
@@ -515,7 +571,7 @@
 
     def finish(k):
         d, s = k // subs, k % subs
-        j = lax.rem(f - half - d + n_fs, n_fs)
+        j = ranked(d)
         slot = j * subs + s
         copy_to(
             pair_recv.at[slot],
@@ -529,17 +585,17 @@
         target = pl.ds(pl.multiple_of(j * part + s * sub_columns, sub_columns), sub_columns)
         result[:, target] = value.astype(jnp.bfloat16)
 
-    for k in range(steps + 3 + subs):
+    for k in range(steps + 4):
         if 2 * subs <= k + 1 < steps:
             spread_relay(1, (k + 1) // subs, (k + 1) % subs)
         if k < steps:
             down_product(k)
         if 0 <= k - 1 < steps:
             to_line(k - 1)
-        if 0 <= k - 2 < steps:
-            to_pair(k - 2)
-        if 0 <= k - 3 - subs < steps:
-            finish(k - 3 - subs)
+        if 0 <= k - 4 < steps:
+            to_pair(k - 4)
+    for k in range(steps):
+        finish(k)
 
     for g in range(2):
         for c in range(chunk_counts[g]):
@@ -547,6 +603,8 @@
             along(g, f, c, 1, drain)
             for p in range(1, n_fs):
                 onward(g, p, c, drain)
+    for g in range(2):
+        spread_own(g, drain)
     for copy in sends:
         copy.wait_send()
 
@@ -574,15 +632,15 @@
         scratch_shapes=[
             pltpu.VMEM((n_fs,) + in_w.shape, bf16),
             pltpu.VMEM((n_fs,) + out_w.shape, bf16),
-            pltpu.VMEM((n_fs, 1, part, half_units), bf16),
-            pltpu.VMEM((n_fs, subs, half_units, sub_columns), bf16),
-            pltpu.VMEM((1, part, half_units), bf16),
-            pltpu.VMEM((subs, half_units, sub_columns), bf16),
+            pltpu.VMEM((n_fs + 1, 1, part, half_units), bf16),
+            pltpu.VMEM((n_fs + 1, subs, half_units, sub_columns), bf16),
             pltpu.VMEM((length, width), bf16),
             pltpu.VMEM((length, channels), f32),
             pltpu.VMEM((length, channels), bf16),
             pltpu.VMEM((n_fs, length, part), bf16),
-            pltpu.VMEM((n_tp, n_fs, rows, part), bf16),
+            pltpu.VMEM((n_fs, n_y, rows, part), bf16),
+            pltpu.VMEM((n_fs, n_y, rows, part), bf16),
+            pltpu.VMEM((n_fs, n_y, rows, part), bf16),
             pltpu.VMEM((n_fs, rows, part), f32),
             pltpu.VMEM((2, length, width), bf16),
             pltpu.VMEM((2, length, half_units), bf16),
@@ -597,10 +655,12 @@
             dma((n_fs, 2 * n_rep + 2, chunks_of(*out_w.shape, n_rep))),
             dma((kinds, n_fs, 1, chunks_of(part, half_units, n_rep))),
             dma((kinds, n_fs, subs, chunks_of(half_units, sub_columns, n_rep))),
-            dma((2, n_tp)),
-            dma((2, n_tp)),
-            dma((n_y + 2, 2, n_tp)),
-            dma((2, n_tp)),
+            dma((n_y + 1, n_tp)),
+            dma((n_tp,)),
+            dma((2, n_fs, n_y)),
+            dma((2, n_fs, n_y)),
+            dma((n_y + 2, 2, n_tp, SHARE_CHUNKS)),
+            dma((2, n_tp, SHARE_CHUNKS)),
             dma((2, steps)),
             dma((2, steps, n_y)),
             dma((2, steps)),

time: 164 us -> 139 us (0.85)
  Pallas kernels: 162 us -> 137 us
    pallas_call x1, Pallas kernels: 162 us -> 137 us  [local(): pl.pallas_call(functools.partial(kernel, sizes), name='layer', out_shape=...]
where the time goes in v2:
time: 139 us
  Pallas kernels  137 us (99%)
  local copies, waits for them, and re-layouts  1.88 us (1%)
    pallas_call x1, Pallas kernels, local(): pl.pallas_call(functools.partial(kernel, sizes), name='layer', out_shape=...  137 us

profile of v2, /device:TPU:0, one launch (start us, length us, event | category | flops | bytes accessed | tf_op | source)
XLA Modules:
  0.0 138.9 jit_solution(3713603215360986916)
XLA Ops:
  0.0 137.0 %layer.1 = bf16[128,2048]{1,0:T(8,128)(2,1)} custom-call(bf16[128,2048]{1,0:T(8,128)(2,1)} %tokens.1, f32[1,2048]{1,0:T(1,128)} %bitcast.3, bf16[512,256]{1,0:T(8,128)(2,1)} %in_hbm.1, bf16[2,128,128]{2,1,0:T(8,128)(2,1)} %group_weight.1, f32[1,256]{1,0:T(1,128)} %bitcast.5, bf16[256,512]{1,0:T(8,128)(2,1)} %out_hbm.1, f32[1,2048]{1,0:T(1,128)} %bitcast.4, ...), custom_call_target="tpu_custom_call" | custom-call | tf_op jit(solution)/shard_map/layer/pallas_call | solution.py:626
  137.0 1.9 %copy.11 = bf16[128,2048]{1,0:T(8,128)(2,1)} copy(bf16[128,2048]{1,0:T(8,128)(2,1)} %layer.1) | data formatting | bytes 1048576

commit v3 on v2

--- a/solution.py
+++ b/solution.py
@@ -9,7 +9,8 @@
 
 MESH = pl.DeviceIdType.MESH
 CHUNK_BYTES = 128 * 1024
-SUB_COLUMNS = 256
+SUB_COLUMNS = 128
+AHEAD = 4
 SHARE_CHUNKS = 4
 LEVELS = 4
 
@@ -69,14 +70,22 @@
     local_sem,
     in_sems,
     out_sems,
-    up_sems,
-    down_sems,
+    up_arrivals,
+    up_swaps,
+    up_sent,
+    down_arrivals,
+    down_swaps,
+    down_sent,
     normed_send,
     normed_recv,
+    mix_sent,
     mix_core_sems,
     mix_line_sems,
-    share_send,
-    share_recv,
+    share_sent,
+    share_core_sems,
+    share_line_sems,
+    share_pair_sems,
+    sums_sent,
     core_sems,
     line_sems,
     pair_sems,
@@ -97,8 +106,11 @@
     half_units = up_buf.shape[3]
     gathered = ((in_buf, in_sems), (out_buf, out_sems))
     chunk_counts = [chunks_of(b.shape[1], b.shape[2], n_rep) for b, _ in gathered]
-    spread = ((up_buf, up_sems), (down_buf, down_sems))
-    spread_counts = [chunks_of(b.shape[2], b.shape[3], n_rep) for b, _ in spread]
+    spread = (
+        (up_buf, up_arrivals, up_swaps, up_sent),
+        (down_buf, down_arrivals, down_swaps, down_sent),
+    )
+    spread_counts = [chunks_of(item[0].shape[2], item[0].shape[3], n_rep) for item in spread]
 
     loads = []
 
@@ -218,12 +230,6 @@
             device_id_type=MESH,
         )
 
-    sends = []
-
-    def send(copy):
-        copy.start()
-        sends.append(copy)
-
     def spread_rows(g, q, c):
         size = spread[g][0].shape[2] // n_rep // spread_counts[g]
         return pl.ds(pl.multiple_of((q * spread_counts[g] + c) * size, size), size)
@@ -235,61 +241,102 @@
         return jnp.where(at_end, order(ends[k - 1]), order(farthest[k - 1]))
 
     def ranked(k):
-        return by_place([1] + farthest[:-1], k) if k else f
+        return order(farthest[k - 1])
+
+    far_steps = [(p, s) for p in range(n_fs - 1, 2, -1) for s in range(subs)]
+    near_steps = [(1, s) for s in range(subs)]
+    next_steps = [(2, s) for s in range(subs)]
+    early = max(1, subs // 2)
+    end_steps = next_steps[:early] + far_steps + near_steps + next_steps[early:]
+    inner_steps = next_steps + far_steps + near_steps
+
+    def step_of(k):
+        if k < subs:
+            return f, k
+        (p, s), (q, u) = end_steps[k - subs], inner_steps[k - subs]
+        return jnp.where(at_end, order(p), order(q)), jnp.where(at_end, s, u)
 
     def sent(k):
         return by_place(farthest[1:2] + farthest[:1] + farthest[2:], k)
 
-    def spread_own(g, act):
-        buf, sems = spread[g]
+    def spread_to(g, to, keep=lambda s, c: True):
+        buf, arrivals, _, sent_sems = spread[g]
+        slot = jnp.where(lax.rem(to, 2) == half, f, n_fs)
+        for s in range(buf.shape[1]):
+            for c in range(spread_counts[g]):
+                if keep(s, c):
+                    piece = spread_rows(g, r, c)
+                    copy_to(
+                        buf.at[slot, s, piece, :],
+                        buf.at[f, s, piece, :],
+                        sent_sems.at[n_rep],
+                        arrivals.at[f, s, c],
+                        {"fs": to},
+                    ).start()
+
+    def spread_own(g, keep=lambda k, c: True):
         for k in range(1, n_fs):
-            to = sent(k)
-            slot = jnp.where(lax.rem(to, 2) == half, f, n_fs)
-            for s in range(buf.shape[1]):
-                for c in range(spread_counts[g]):
-                    piece = spread_rows(g, r, c)
-                    act(
-                        copy_to(
-                            buf.at[slot, s, piece, :],
-                            buf.at[f, s, piece, :],
-                            sems.at[0, to, s, c],
-                            sems.at[1, f, s, c],
-                            {"fs": to},
-                        )
-                    )
-
-    def spread_relay(g, k, s):
-        buf, sems = spread[g]
-        j = ranked(k)
-        for c in range(spread_counts[g]):
+            spread_to(g, sent(k), lambda s, c: keep(k, c))
+
+    def spread_late(g):
+        def opening(s, c):
+            return s == 0 and c == 0
+
+        def rest(s, c):
+            return not opening(s, c)
+
+        @pl.when(at_end)
+        def _():
+            spread_to(g, order(1))
+            for p in range(n_fs - 1, 1, -1):
+                spread_to(g, order(p))
+
+        @pl.when(jnp.logical_not(at_end))
+        def _():
+            spread_to(g, order(1), opening)
+            for p in range(n_fs - 1, 2, -1):
+                spread_to(g, order(p))
+            spread_to(g, order(1), rest)
+            spread_to(g, order(2))
+
+    def spread_relay(g, j, s, chunks=None):
+        buf, arrivals, swaps, sent_sems = spread[g]
+        for c in range(spread_counts[g]) if chunks is None else chunks:
             block = buf.at[j, s, spread_rows(g, r, c), :]
-            copy_to(block, block, sems.at[0, j, s, c], sems.at[1, j, s, c], {"fs": j}).wait_recv()
+            copy_to(block, block, sent_sems.at[n_rep], arrivals.at[j, s, c], {"fs": j}).wait_recv()
             for e in range(1, n_rep):
                 other = lax.rem(r + e, n_rep)
-                send(
-                    copy_to(
-                        block,
-                        block,
-                        sems.at[2 + other, j, s, c],
-                        sems.at[2 + n_rep + r, j, s, c],
-                        {"rep": other},
-                    )
-                )
-
-    def spread_arrived(g, k, s):
-        buf, sems = spread[g]
-        j = ranked(k)
+                copy_to(
+                    block, block, sent_sems.at[other], swaps.at[r, j, s], {"rep": other}
+                ).start()
+
+    def share_of(g, q):
+        size = spread[g][0].shape[2] // n_rep
+        return pl.ds(pl.multiple_of(q * size, size), size)
+
+    def spread_arrived(g, j, s):
+        buf, _, swaps, sent_sems = spread[g]
         for e in range(1, n_rep):
             other = lax.rem(r + e, n_rep)
-            for c in range(spread_counts[g]):
-                block = buf.at[j, s, spread_rows(g, other, c), :]
-                copy_to(
-                    block,
-                    block,
-                    sems.at[2 + other, j, s, c],
-                    sems.at[2 + n_rep + other, j, s, c],
-                    {"rep": other},
-                ).wait_recv()
+            block = buf.at[j, s, share_of(g, other), :]
+            copy_to(
+                block, block, sent_sems.at[other], swaps.at[other, j, s], {"rep": other}
+            ).wait_recv()
+
+    def spread_drain(g):
+        buf, arrivals, _, sent_sems = spread[g]
+        block = buf.at[: n_fs - 1, :, share_of(g, 0), :]
+        for e in range(1, n_rep):
+            other = lax.rem(r + e, n_rep)
+            copy_to(
+                block, block, sent_sems.at[other], arrivals.at[0, 0, 0], {"rep": other}
+            ).wait_send()
+        copy_to(
+            block, block, sent_sems.at[n_rep], arrivals.at[0, 0, 0], {"tp": t_pair}
+        ).wait_send()
+
+    def drained(block, sem):
+        copy_to(block, block, sem, sem, {"tp": t_pair}).wait_send()
 
     stream = tokens[...].astype(jnp.float32)
     scale = lax.rsqrt(jnp.mean(stream * stream, axis=-1, keepdims=True) + epsilon)
@@ -300,16 +347,16 @@
 
     def give_normed(owner, slot, device):
         block = normed.at[block_of(owner), :]
-        return copy_to(block, block, normed_send.at[slot, owner], normed_recv.at[owner], device)
+        return copy_to(block, block, normed_send.at[slot], normed_recv.at[owner], device)
 
     def normed_from(owner):
-        give_normed(owner, n_y, {"tp": t_pair}).wait_recv()
+        give_normed(owner, 1, {"tp": t_pair}).wait_recv()
 
     pl.semaphore_wait(barrier, len(greeted))
     for e in range(1, n_y):
         to = on_line(e)
-        send(give_normed(t, to, {"tp": 2 * to + core}))
-    send(give_normed(t, n_y, {"tp": t_pair}))
+        give_normed(t, 0, {"tp": 2 * to + core}).start()
+    give_normed(t, 1, {"tp": t_pair}).start()
     loads[0].wait()
     send_own(0)
     loads[1].wait()
@@ -321,13 +368,20 @@
     for e in range(1, n_y):
         owner = 2 * on_line(e) + core
         normed_from(owner)
-        send(give_normed(owner, n_y, {"tp": t_pair}))
+        give_normed(owner, 1, {"tp": t_pair}).start()
     for copy in loads[2:]:
         copy.wait()
 
+    def first_part(k, c):
+        return k == 2 and c < spread_counts[0] // 2
+
     @pl.when(at_end)
     def _():
-        spread_own(0, start)
+        spread_own(0)
+
+    @pl.when(jnp.logical_not(at_end))
+    def _():
+        spread_own(0, first_part)
 
     for p in range(1, n_fs):
         arrived(0, p)
@@ -354,24 +408,22 @@
         mapped = dot(pooled, group_weight[group])
         pool_out[:, lanes] = (mapped * pool_scale[:, lanes]).astype(jnp.bfloat16)
 
-
     @pl.when(jnp.logical_not(at_end))
     def _():
-        spread_own(0, start)
+        spread_own(0, lambda k, c: not first_part(k, c))
 
     for p in range(1, n_fs):
         arrived(1, p)
+
     def mix_by_core(index, e):
         block = mix_send.at[index, block_of(2 * e + 1 - core), :]
-        sems = mix_core_sems
         return copy_to(
-            block, mix_core.at[index, e], sems.at[0, index, e], sems.at[1, index, e], {"tp": t_pair}
+            block, mix_core.at[index, e], mix_sent.at[0], mix_core_sems.at[index], {"tp": t_pair}
         )
 
-    def mix_by_line(index, source, target, to):
-        sems = mix_line_sems
+    def mix_by_line(index, source, target, e, to):
         return copy_to(
-            source, target, sems.at[0, index, to], sems.at[1, index, y], {"tp": 2 * to + core}
+            source, target, mix_sent.at[1], mix_line_sems.at[index, e], {"tp": 2 * to + core}
         )
 
     def mix_pair(index, which):
@@ -381,29 +433,27 @@
     for index in range(n_fs):
         mix_send[index] = dot(pool_out[...], out_buf[index]).astype(jnp.bfloat16)
         for e in range(n_y):
-            send(mix_by_core(index, e))
+            mix_by_core(index, e).start()
     for index in range(n_fs):
-        for e in range(n_y):
-            mix_by_core(index, e).wait_recv()
+        block = mix_core.at[index]
+        copy_to(block, block, mix_sent.at[0], mix_core_sems.at[index], {"tp": t_pair}).wait_recv()
         for e in range(1, n_y):
             to = on_line(e)
             mix_line_send[index, to] = mix_pair(index, to).astype(jnp.bfloat16)
-            send(mix_by_line(index, mix_line_send.at[index, to], mix_line.at[index, y], to))
-
-    spread_relay(0, 1, 0)
+            source, target = mix_line_send.at[index, to], mix_line.at[index, y]
+            mix_by_line(index, source, target, n_y - e - 1, to).start()
+
+    @pl.when(jnp.logical_not(at_end))
+    def _():
+        spread_relay(0, ranked(1), 0)
+
     square = jnp.zeros((rows, 1), jnp.float32)
     for index in range(n_fs):
         mixed = tokens[:, index * part : (index + 1) * part].astype(jnp.float32)
         mixed += mix_pair(index, y)
         for e in range(1, n_y):
             block = mix_line.at[index, on_line(e)]
-            copy_to(
-                block,
-                block,
-                mix_line_sems.at[0, index, on_line(e)],
-                mix_line_sems.at[1, index, on_line(e)],
-                {"tp": t_pair},
-            ).wait_recv()
+            mix_by_line(index, block, block, e - 1, on_line(e)).wait_recv()
             mixed += block[...].astype(jnp.float32)
         stream2[index] = mixed
         square += jnp.sum(mixed * mixed, axis=-1, keepdims=True)
@@ -418,61 +468,79 @@
             jnp.bfloat16
         )
 
-    def share(plane, owner, c, send_slot, device):
+    def share(plane, owner, c, sent_sem, sem, device):
         size = rows // SHARE_CHUNKS
         place = lax.rem(owner, 2) * n_y + owner // 2
         start = pl.multiple_of(place * rows + c * size, size)
         block = shared.at[plane, pl.ds(start, size), :]
-        return copy_to(
-            block,
-            block,
-            share_send.at[send_slot, plane, owner, c],
-            share_recv.at[plane, owner, c],
-            device,
-        )
+        return copy_to(block, block, share_sent.at[sent_sem], sem, device)
 
     def share_core(plane, owner, c):
-        send(share(plane, owner, c, n_y, {"tp": t_pair}))
+        share(plane, owner, c, 0, share_core_sems.at[plane], {"tp": t_pair}).start()
+
+    def by_line(plane, owner, c, e, to):
+        sem = share_line_sems.at[plane, e, c]
+        return share(plane, owner, c, 1, sem, {"tp": 2 * to + core})
 
     def share_line(plane, c):
         for e in range(1, n_y):
-            to = on_line(e)
-            send(share(plane, t, c, to, {"tp": 2 * to + core}))
-
-    def shared_from(plane, owner, c):
-        share(plane, owner, c, n_y, {"tp": t_pair}).wait_recv()
+            by_line(plane, t, c, n_y - e - 1, on_line(e)).start()
+
+    def pass_line(plane, c):
+        for e in range(1, n_y):
+            owner = 2 * on_line(e) + core
+            by_line(plane, owner, c, e - 1, on_line(e)).wait_recv()
+            share_core(plane, owner, c)
+
+    def by_pair(plane, c):
+        return share(plane, t, c, 2, share_pair_sems.at[c], {"fs": f_pair})
 
     def shared_by_core(plane):
-        for e in range(n_y):
-            for c in range(SHARE_CHUNKS):
-                shared_from(plane, 2 * on_line(e) + 1 - core, c)
+        block = shared.at[plane, block_rows(1 - core), :]
+        copy_to(
+            block, block, share_sent.at[0], share_core_sems.at[plane], {"tp": t_pair}
+        ).wait_recv()
+
+    line_rows = n_y * rows
+
+    def block_rows(which):
+        return pl.ds(pl.multiple_of(which * line_rows, line_rows), line_rows)
 
     for c in range(SHARE_CHUNKS):
-        send(share(half, t, c, n_y + 1, {"fs": f_pair}))
+        by_pair(half, c).start()
         share_line(half, c)
         share_core(half, t, c)
-    spread_own(1, start)
+    spread_late(1)
+
+    @pl.when(at_end)
+    def _():
+        spread_relay(0, ranked(1), 0)
+
     for c in range(SHARE_CHUNKS):
-        for e in range(1, n_y):
-            owner = 2 * on_line(e) + core
-            shared_from(half, owner, c)
-            share_core(half, owner, c)
+        pass_line(half, c)
     for k in range(2, n_fs - 1):
-        spread_relay(0, k, 0)
+        spread_relay(0, ranked(k), 0)
+
+    @pl.when(at_end)
+    def _():
+        spread_relay(0, ranked(n_fs - 1), 0)
+
+    last_chunks = spread_counts[0]
     for c in range(SHARE_CHUNKS):
-        shared_from(1 - half, t, c)
+        by_pair(1 - half, c).wait_recv()
         share_line(1 - half, c)
         share_core(1 - half, t, c)
-    spread_relay(0, n_fs - 1, 0)
+        begin, end = c * last_chunks // SHARE_CHUNKS, (c + 1) * last_chunks // SHARE_CHUNKS
+
+        @pl.when(jnp.logical_not(at_end))
+        def _():
+            spread_relay(0, ranked(n_fs - 1), 0, range(begin, end))
+
     for c in range(SHARE_CHUNKS):
-        for e in range(1, n_y):
-            owner = 2 * on_line(e) + core
-            shared_from(1 - half, owner, c)
-            share_core(1 - half, owner, c)
+        pass_line(1 - half, c)
     shared_by_core(half)
-    spread_relay(1, 1, 0)
     for d in range(1, n_fs):
-        spread_arrived(0, d, 0)
+        spread_arrived(0, ranked(d), 0)
 
     up_tile = tile_of(half_units, 256)
 
@@ -487,66 +555,61 @@
             value = jnp.maximum(total, 0.0)
             hidden[plane, :, columns] = (value * value).astype(jnp.bfloat16)
 
+    relayed = [subs]
+
+    def relay_steps(upto):
+        while relayed[0] < min(upto, steps):
+            j, s = step_of(relayed[0])
+            relayed[0] += 1
+            spread_relay(1, j, s)
+
+    relay_steps(subs + subs // 2)
     up_product(half)
-    for s in range(1, subs):
-        spread_relay(1, 1, s)
+    relay_steps(2 * subs - 1)
     shared_by_core(1 - half)
     up_product(1 - half)
 
-    line_rows = n_y * rows
-
-    def own_rows(which):
-        return pl.ds(pl.multiple_of(which * line_rows, line_rows), line_rows)
+    def columns_of(s):
+        return pl.ds(pl.multiple_of(s * sub_columns, sub_columns), sub_columns)
 
     def down_product(k):
-        d, s = k // subs, k % subs
-        j = ranked(d)
-        if d:
-            spread_arrived(1, d, s)
+        j, s = step_of(k)
+        if k >= subs:
+            spread_arrived(1, j, s)
         for plane in range(2):
             product = dot(hidden[plane], down_buf[j, s])
             core_send[k, plane] = product.astype(jnp.bfloat16)
-        send(
-            copy_to(
-                core_send.at[k, :, own_rows(1 - core), :],
-                core_recv.at[k],
-                core_sems.at[0, k],
-                core_sems.at[1, k],
-                {"tp": t_pair},
-            )
-        )
+        copy_to(
+            core_send.at[k, :, block_rows(1 - core), :],
+            core_recv.at[k],
+            sums_sent.at[0],
+            core_sems.at[k],
+            {"tp": t_pair},
+        ).start()
 
     def to_line(k):
-        copy_to(
-            core_recv.at[k], core_recv.at[k], core_sems.at[0, k], core_sems.at[1, k], {"tp": t_pair}
-        ).wait_recv()
+        block = core_recv.at[k]
+        copy_to(block, block, sums_sent.at[0], core_sems.at[k], {"tp": t_pair}).wait_recv()
         for plane in range(2):
-            own = core_send[k, plane, own_rows(core), :].astype(jnp.float32)
+            own = core_send[k, plane, block_rows(core), :].astype(jnp.float32)
             both = own + core_recv[k, plane].astype(jnp.float32)
             line_send[k, plane] = both.astype(jnp.bfloat16)
         for e in range(1, n_y):
             to = on_line(e)
-            send(
-                copy_to(
-                    line_send.at[k, :, block_of(to), :],
-                    line_recv.at[k, y],
-                    line_sems.at[0, k, to],
-                    line_sems.at[1, k, y],
-                    {"tp": 2 * to + core},
-                )
-            )
+            copy_to(
+                line_send.at[k, :, block_of(to), :],
+                line_recv.at[k, y],
+                sums_sent.at[1],
+                line_sems.at[k, n_y - e - 1],
+                {"tp": 2 * to + core},
+            ).start()
 
     def to_pair(k):
-        d, s = k // subs, k % subs
-        j = ranked(d)
+        j, s = step_of(k)
         for e in range(1, n_y):
             block = line_recv.at[k, on_line(e)]
             copy_to(
-                block,
-                block,
-                line_sems.at[0, k, on_line(e)],
-                line_sems.at[1, k, on_line(e)],
-                {"tp": t_pair},
+                block, block, sums_sent.at[1], line_sems.at[k, e - 1], {"tp": t_pair}
             ).wait_recv()
 
         def total_of(plane):
@@ -557,56 +620,54 @@
             return total
 
         pair_send[j * subs + s] = total_of(1 - half).astype(jnp.bfloat16)
-        send(
-            copy_to(
-                pair_send.at[j * subs + s],
-                pair_recv.at[j * subs + s],
-                pair_sems.at[0, j * subs + s],
-                pair_sems.at[1, j * subs + s],
-                {"fs": f_pair},
-            )
-        )
-        columns = slice(s * sub_columns, (s + 1) * sub_columns)
-        stream2[j, :, columns] += total_of(half)
-
-    def finish(k):
-        d, s = k // subs, k % subs
-        j = ranked(d)
         slot = j * subs + s
         copy_to(
+            pair_send.at[slot],
             pair_recv.at[slot],
-            pair_recv.at[slot],
-            pair_sems.at[0, slot],
-            pair_sems.at[1, slot],
+            sums_sent.at[2],
+            pair_sems.at[slot],
             {"fs": f_pair},
-        ).wait_recv()
-        columns = slice(s * sub_columns, (s + 1) * sub_columns)
+        ).start()
+        columns = columns_of(s)
+        stream2[j, :, columns] += total_of(half)
+
+    def finish(k):
+        j, s = step_of(k)
+        slot = j * subs + s
+        block = pair_recv.at[slot]
+        copy_to(block, block, sums_sent.at[2], pair_sems.at[slot], {"fs": f_pair}).wait_recv()
+        columns = columns_of(s)
         value = stream2[j, :, columns] + pair_recv[slot].astype(jnp.float32)
         target = pl.ds(pl.multiple_of(j * part + s * sub_columns, sub_columns), sub_columns)
         result[:, target] = value.astype(jnp.bfloat16)
 
     for k in range(steps + 4):
-        if 2 * subs <= k + 1 < steps:
-            spread_relay(1, (k + 1) // subs, (k + 1) % subs)
+        relay_steps(k + AHEAD + 1)
         if k < steps:
             down_product(k)
         if 0 <= k - 1 < steps:
             to_line(k - 1)
         if 0 <= k - 4 < steps:
             to_pair(k - 4)
-    for k in range(steps):
-        finish(k)
-
     for g in range(2):
+        spread_drain(g)
         for c in range(chunk_counts[g]):
             along(g, f, c, 0, drain)
             along(g, f, c, 1, drain)
             for p in range(1, n_fs):
                 onward(g, p, c, drain)
-    for g in range(2):
-        spread_own(g, drain)
-    for copy in sends:
-        copy.wait_send()
+    drained(normed.at[: line_rows - rows, :], normed_send.at[0])
+    drained(normed.at[:line_rows, :], normed_send.at[1])
+    drained(mix_core, mix_sent.at[0])
+    drained(mix_line.at[:, : n_y - 1], mix_sent.at[1])
+    drained(shared.at[:, :line_rows, :], share_sent.at[0])
+    drained(shared.at[:, : line_rows - rows, :], share_sent.at[1])
+    drained(shared.at[0, :rows, :], share_sent.at[2])
+    drained(core_recv, sums_sent.at[0])
+    drained(line_recv.at[:, : n_y - 1], sums_sent.at[1])
+    for k in range(steps):
+        finish(k)
+    drained(pair_recv, sums_sent.at[2])
 
 
 def local(sizes, tokens, gain1, in_w, group_w, pool_scale, out_w, gain2, up_w, down_w):
@@ -622,7 +683,6 @@
     vmem = pl.BlockSpec(memory_space=pltpu.VMEM)
     hbm = pl.BlockSpec(memory_space=pl.ANY)
     dma = pltpu.SemaphoreType.DMA
-    kinds = 2 + 2 * n_rep
     return pl.pallas_call(
         functools.partial(kernel, sizes),
         name="layer",
@@ -653,17 +713,25 @@
             dma((4 + 2 * subs,)),
             dma((n_fs, 2 * n_rep + 2, chunks_of(*in_w.shape, n_rep))),
             dma((n_fs, 2 * n_rep + 2, chunks_of(*out_w.shape, n_rep))),
-            dma((kinds, n_fs, 1, chunks_of(part, half_units, n_rep))),
-            dma((kinds, n_fs, subs, chunks_of(half_units, sub_columns, n_rep))),
-            dma((n_y + 1, n_tp)),
+            dma((n_fs, 1, chunks_of(part, half_units, n_rep))),
+            dma((n_rep, n_fs, 1)),
+            dma((n_rep + 1,)),
+            dma((n_fs, subs, chunks_of(half_units, sub_columns, n_rep))),
+            dma((n_rep, n_fs, subs)),
+            dma((n_rep + 1,)),
+            dma((2,)),
             dma((n_tp,)),
-            dma((2, n_fs, n_y)),
-            dma((2, n_fs, n_y)),
-            dma((n_y + 2, 2, n_tp, SHARE_CHUNKS)),
-            dma((2, n_tp, SHARE_CHUNKS)),
-            dma((2, steps)),
-            dma((2, steps, n_y)),
-            dma((2, steps)),
+            dma((2,)),
+            dma((n_fs,)),
+            dma((n_fs, n_y - 1)),
+            dma((3,)),
+            dma((2,)),
+            dma((2, n_y - 1, SHARE_CHUNKS)),
+            dma((SHARE_CHUNKS,)),
+            dma((3,)),
+            dma((steps,)),
+            dma((steps, n_y - 1)),
+            dma((steps,)),
         ],
         compiler_params=pltpu.CompilerParams(
             collective_id=0, has_side_effects=True, vmem_limit_bytes=60 * 1024 * 1024

time: 139 us -> 136 us (0.978)
  Pallas kernels: 137 us -> 134 us
    pallas_call x1, Pallas kernels: 137 us -> 134 us  [local(): pl.pallas_call(functools.partial(kernel, sizes), name='layer', out_shape=...]
where the time goes in v3:
time: 136 us
  Pallas kernels  134 us (99%)
  local copies, waits for them, and re-layouts  1.88 us (1%)
    pallas_call x1, Pallas kernels, local(): pl.pallas_call(functools.partial(kernel, sizes), name='layer', out_shape=...  134 us

profile of v3, /device:TPU:0, one launch (start us, length us, event | category | flops | bytes accessed | tf_op | source)
XLA Modules:
  0.0 136.0 jit_solution(11255581983052256335)
XLA Ops:
  0.0 134.1 %layer.1 = bf16[128,2048]{1,0:T(8,128)(2,1)} custom-call(bf16[128,2048]{1,0:T(8,128)(2,1)} %tokens.1, f32[1,2048]{1,0:T(1,128)} %bitcast.3, bf16[512,256]{1,0:T(8,128)(2,1)} %in_hbm.1, bf16[2,128,128]{2,1,0:T(8,128)(2,1)} %group_weight.1, f32[1,256]{1,0:T(1,128)} %bitcast.5, bf16[256,512]{1,0:T(8,128)(2,1)} %out_hbm.1, f32[1,2048]{1,0:T(1,128)} %bitcast.4, ...), custom_call_target="tpu_custom_call" | custom-call | tf_op jit(solution)/shard_map/layer/pallas_call | solution.py:686
  134.1 1.9 %copy.11 = bf16[128,2048]{1,0:T(8,128)(2,1)} copy(bf16[128,2048]{1,0:T(8,128)(2,1)} %layer.1) | data formatting | bytes 1048576

commit v4 on v3

--- a/solution.py
+++ b/solution.py
@@ -9,8 +9,8 @@
 
 MESH = pl.DeviceIdType.MESH
 CHUNK_BYTES = 128 * 1024
-SUB_COLUMNS = 128
-AHEAD = 4
+SUB_COLUMNS = 256
+AHEAD = 2
 SHARE_CHUNKS = 4
 LEVELS = 4
 

time: 136 us -> 136 us (level)
  no operation moved by 1% of the time
where the time goes in v4:
time: 136 us
  Pallas kernels  134 us (99%)
  local copies, waits for them, and re-layouts  1.88 us (1%)
    pallas_call x1, Pallas kernels, local(): pl.pallas_call(functools.partial(kernel, sizes), name='layer', out_shape=...  134 us

profile of v4, /device:TPU:0, one launch (start us, length us, event | category | flops | bytes accessed | tf_op | source)
XLA Modules:
  0.0 135.7 jit_solution(3899716693693779944)
XLA Ops:
  0.0 133.8 %layer.1 = bf16[128,2048]{1,0:T(8,128)(2,1)} custom-call(bf16[128,2048]{1,0:T(8,128)(2,1)} %tokens.1, f32[1,2048]{1,0:T(1,128)} %bitcast.3, bf16[512,256]{1,0:T(8,128)(2,1)} %in_hbm.1, bf16[2,128,128]{2,1,0:T(8,128)(2,1)} %group_weight.1, f32[1,256]{1,0:T(1,128)} %bitcast.5, bf16[256,512]{1,0:T(8,128)(2,1)} %out_hbm.1, f32[1,2048]{1,0:T(1,128)} %bitcast.4, ...), custom_call_target="tpu_custom_call" | custom-call | tf_op jit(solution)/shard_map/layer/pallas_call | solution.py:686
  133.8 1.9 %copy.11 = bf16[128,2048]{1,0:T(8,128)(2,1)} copy(bf16[128,2048]{1,0:T(8,128)(2,1)} %layer.1) | data formatting | bytes 1048576
